TPU v7x, 32 devices: a whole 2x2x4 slice. The times are simulated.
32 devices in a mesh: grp: 2 (over y), fs: 4 (over z), tp: 4 (over x, core).
Axes of the slice: x: 2, y: 2, z: 4, core: 2. Of those that a mesh axis runs over, the one named last changes fastest.
Arguments:
- tokens: bfloat16 [8192, 2048], P(('grp', 'fs', 'tp')), parts along dimension 0, may hold values from -6 to 6
- first_gain: float32 [2048], replicated, may hold values from 0.1 to 1.9
- mixer_gain: float32 [2048], replicated, may hold values from 0.1 to 1.9
- gate_weight: bfloat16 [2048, 4608], P('fs', 'tp'), may hold values from -0.125 to 0.125
- up_weight: bfloat16 [2048, 4608], P('fs', 'tp'), may hold values from -0.125 to 0.125
- down_weight: bfloat16 [4608, 2048], P('tp', 'fs'), may hold values from -0.09375 to 0.09375
- query_weight: bfloat16 [2048, 2048], P('fs', 'tp'), may hold values from -0.125 to 0.125
- key_weight: bfloat16 [2048, 2048], P('fs', 'tp'), may hold values from -0.125 to 0.125
- value_weight: bfloat16 [2048, 4096], P('fs', 'tp'), may hold values from -0.125 to 0.125
- head_gain: float32 [4096], P('tp'), may hold values from 0.1 to 1.9
- out_weight: bfloat16 [4096, 2048], P('tp', 'fs'), may hold values from -0.09375 to 0.09375
- log_decay: float32 [2, 8], P(None, 'tp'), may hold values from -0.03125 to 0, as said below
Outputs:
- updated: bfloat16 [8192, 2048], P(('grp', 'fs', 'tp')), parts along dimension 0
There are 2 independent parts, one for each index of `grp`. A program takes and returns all parts, laid end to end along the dimension named above; an argument that names none is the same for every part. Nothing has to cross between parts.
Inputs may be any that keep to these rules, and one draw needn't show every extreme that they name: `log_decay`: log decay per step of each direction (forward, then backward) and head.
All inputs are finite; a program needn't handle non-finite values.
Results may differ from a plain program's by a relative error of at most 0.02.
Values may be sent and summed in bfloat16 or wider, within the bound.
No kernel may reach another device: no remote copies, remote signals or barrier semaphores. Data moves between devices by JAX's collectives and lax.ppermute only.
A program may use at most 64 MiB of HBM per device.

v0:
```python
import jax
import jax.numpy as jnp
from jax import lax
from jax.sharding import PartitionSpec as P

DK = 256
DV = 512
BLOCK = 128


EPS = 1e-06


def norm_rows(values, gain):
    widened = values.astype(jnp.float32)
    factor = lax.rsqrt(jnp.mean(widened * widened, axis=-1, keepdims=True) + EPS)
    return (widened * factor * gain).astype(jnp.bfloat16)


def sweep_one(queries, key_rows, value_rows, log_rate):
    length = queries.shape[0]
    block_count = length // BLOCK
    places = jnp.arange(BLOCK, dtype=jnp.float32)
    distance = places[:, None] - places[None, :]
    inner_decay = jnp.where(distance >= 0, jnp.exp(log_rate * jnp.maximum(distance, 0.0)), 0.0)
    enter_decay = jnp.exp(log_rate * (places + 1.0))
    leave_decay = jnp.exp(log_rate * (BLOCK - 1.0 - places))
    block_decay = jnp.exp(log_rate * BLOCK)
    highest = lax.Precision.HIGHEST

    def advance(memory, blocks):
        query_block, key_block, value_block = blocks
        scores = (
            jnp.dot(
                query_block.astype(jnp.bfloat16),
                key_block.astype(jnp.bfloat16).T,
                preferred_element_type=jnp.float32,
            )
            * inner_decay
        )
        result = jnp.dot(scores, value_block, precision=highest)
        result = result + jnp.dot(query_block, memory, precision=highest) * enter_decay[:, None]
        memory = memory * block_decay + jnp.dot(
            (key_block * leave_decay[:, None]).T, value_block, precision=highest
        )
        return (memory, result)

    start_memory = jnp.zeros((queries.shape[1], value_rows.shape[1]), jnp.float32)
    _, results = lax.scan(
        advance,
        start_memory,
        (
            queries.reshape(block_count, BLOCK, -1),
            key_rows.reshape(block_count, BLOCK, -1),
            value_rows.reshape(block_count, BLOCK, -1),
        ),
    )
    return results.reshape(length, -1)


def retain_both(queries, key_rows, value_rows, forward_rate, backward_rate):
    forward_part = sweep_one(queries, key_rows, value_rows, forward_rate)
    backward_part = sweep_one(
        jnp.flip(queries, axis=0),
        jnp.flip(key_rows, axis=0),
        jnp.flip(value_rows, axis=0),
        backward_rate,
    )
    return forward_part + jnp.flip(backward_part, axis=0)


def head_norm(outputs, gain):
    heads_here = gain.shape[0] // DV
    centered = outputs - jnp.mean(outputs, axis=-1, keepdims=True)
    variance = jnp.mean(centered * centered, axis=-1, keepdims=True)
    return centered * lax.rsqrt(variance + EPS) * gain.reshape(heads_here, 1, DV)


def to_heads(values, width):
    widened = lax.optimization_barrier(values.astype(jnp.bfloat16)).astype(jnp.float32)
    return widened.reshape(values.shape[0], -1, width).transpose(1, 0, 2)


def feed_half(residual, gain, gate_weight, up_weight, down_weight):
    normed = norm_rows(residual, gain)
    gathered = lax.all_gather(normed, "tp", axis=0, tiled=True)
    gate_sum = jnp.dot(
        gathered,
        lax.all_gather(gate_weight, "fs", axis=0, tiled=True),
        preferred_element_type=jnp.float32,
    )
    up_sum = jnp.dot(
        gathered,
        lax.all_gather(up_weight, "fs", axis=0, tiled=True),
        preferred_element_type=jnp.float32,
    )
    hidden = (jax.nn.silu(gate_sum) * up_sum).astype(jnp.bfloat16)
    partial_out = jnp.dot(
        hidden,
        lax.all_gather(down_weight, "fs", axis=1, tiled=True),
        preferred_element_type=jnp.float32,
    )
    summed = lax.psum_scatter(
        partial_out.astype(jnp.bfloat16), "tp", scatter_dimension=0, tiled=True
    ).astype(jnp.float32)
    return (residual.astype(jnp.float32) + 0.5 * summed).astype(jnp.bfloat16)


def mix_tokens(
    residual, gain, query_weight, key_weight, value_weight, head_gain, out_weight, log_decay
):
    normed = norm_rows(residual, gain)
    gathered = lax.all_gather(normed, "tp", axis=0, tiled=True)
    rows_here = gathered.shape[0]
    segments = (
        lax.all_gather(query_weight, "fs", axis=0, tiled=True),
        lax.all_gather(key_weight, "fs", axis=0, tiled=True),
        lax.all_gather(value_weight, "fs", axis=0, tiled=True),
    )
    query_sum, key_sum, value_sum = tuple(
        (jnp.dot(gathered, segment, preferred_element_type=jnp.float32) for segment in segments)
    )
    queries = to_heads(query_sum, DK) * DK ** (-0.5)
    key_rows = to_heads(key_sum, DK)
    value_rows = to_heads(value_sum, DV)
    outputs = jax.vmap(retain_both)(queries, key_rows, value_rows, log_decay[0], log_decay[1])
    normed_heads = head_norm(outputs, head_gain).astype(jnp.bfloat16)
    flat = normed_heads.transpose(1, 0, 2).reshape(rows_here, -1)
    partial_out = jnp.dot(
        flat,
        lax.all_gather(out_weight, "fs", axis=1, tiled=True),
        preferred_element_type=jnp.float32,
    )
    summed = lax.psum_scatter(
        partial_out.astype(jnp.bfloat16), "tp", scatter_dimension=0, tiled=True
    ).astype(jnp.float32)
    return (residual.astype(jnp.float32) + summed).astype(jnp.bfloat16)


def shards(
    tokens,
    first_gain,
    mixer_gain,
    gate_weight,
    up_weight,
    down_weight,
    query_weight,
    key_weight,
    value_weight,
    head_gain,
    out_weight,
    log_decay,
):
    after_first = feed_half(tokens, first_gain, gate_weight, up_weight, down_weight)
    return mix_tokens(
        after_first,
        mixer_gain,
        query_weight,
        key_weight,
        value_weight,
        head_gain,
        out_weight,
        log_decay,
    )


def solution(mesh):
    placed = (
        P(("grp", "fs", "tp"), None),
        P(),
        P(),
        P("fs", "tp"),
        P("fs", "tp"),
        P("tp", "fs"),
        P("fs", "tp"),
        P("fs", "tp"),
        P("fs", "tp"),
        P("tp"),
        P("tp", "fs"),
        P(None, "tp"),
    )
    return jax.shard_map(
        shards, mesh=mesh, in_specs=placed, out_specs=P(("grp", "fs", "tp"), None), check_vma=False
    )
```

profile of v0, /device:TPU:0, one launch (start us, length us, event | category | flops | bytes accessed | tf_op | source)
XLA Modules:
  0.0 909.5 jit_solution(16206090726503417399)
XLA Ops:
  8.1 2.5 fusion.53
  12.7 35.2 %all-gather.10.cloned.1.call-done = bf16[1024,2048]{1,0:T(8,128)(2,1)} async-done(((bf16[256,2048]{1,0:T(8,128)(2,1)}), bf16[1024,2048]{1,0:T(8,128)(2,1)}) %all-gather.10.cloned.1.call-update) | async-done | bytes 4194320 | tf_op jit(solution)/shard_map/all_gather | solution.py:86
  47.9 91.0 %all-gather.12.cloned.1.call-done = bf16[2048,1152]{1,0:T(8,128)(2,1)} async-done(((bf16[512,1152]{1,0:T(8,128)(2,1)}), bf16[2048,1152]{1,0:T(8,128)(2,1)}) %all-gather.12.cloned.1.call-update) | async-done | bytes 4718608 | tf_op jit(solution)/shard_map/all_gather | solution.py:89
  138.9 10.2 %fusion.72 = f32[1024,1152]{1,0:T(8,128)} fusion(bf16[1024,2048]{1,0:T(8,128)(2,1)} %all-gather.10.cloned.1.call-done, bf16[2048,1152]{1,0:T(8,128)(2,1)} %all-gather.12.cloned.1.call-done), kind=kOutput, calls=%fused_computation.111 | convolution fusion | flops 4831838208 | bytes 13631488 | tf_op jit(solution)/shard_map/dot_general | solution.py:87
  149.1 79.2 %all-gather.14.cloned.1.call-done = bf16[2048,1152]{1,0:T(8,128)(2,1)} async-done(((bf16[512,1152]{1,0:T(8,128)(2,1)}), bf16[2048,1152]{1,0:T(8,128)(2,1)}) %all-gather.14.cloned.1.call-update) | async-done | bytes 4718608 | tf_op jit(solution)/shard_map/all_gather | solution.py:94
  228.3 89.3 %all-gather.16.cloned.1.call-done = bf16[1152,2048]{1,0:T(8,128)(2,1)} async-done(((bf16[1152,512]{1,0:T(8,128)(2,1)}), bf16[1152,2048]{1,0:T(8,128)(2,1)}) %all-gather.16.cloned.1.call-update) | async-done | bytes 4718608 | tf_op jit(solution)/shard_map/all_gather | solution.py:100
  317.6 19.2 %convolution_convert_fusion = bf16[1024,2048]{1,0:T(8,128)(2,1)} fusion(bf16[1152,2048]{1,0:T(8,128)(2,1)} %all-gather.16.cloned.1.call-done, bf16[1024,2048]{1,0:T(8,128)(2,1)} %all-gather.10.cloned.1.call-done, bf16[2048,1152]{1,0:T(8,128)(2,1)} %all-gather.14.cloned.1.call-done, f32[1024,1152]{1,0:T(8,128)} %fusion.72), kind=kOutput, calls=%fused_computation.68 | convolution fusion | flops 9672851456 | bytes 22544384 | tf_op jit(solution)/shard_map/dot_general | solution.py:98
  337.4 42.5 %reduce-scatter.3.cloned.1.call-done = bf16[256,2048]{1,0:T(8,128)(2,1)} async-done(((bf16[1024,2048]{1,0:T(8,128)(2,1)}), bf16[256,2048]{1,0:T(8,128)(2,1)}) %reduce-scatter.3.cloned.1.call-update) | async-done | bytes 1048592 | tf_op jit(solution)/shard_map/reduce_scatter | solution.py:103
  379.9 1.7 fusion.55
  381.6 2.7 fusion.57
  386.8 40.2 %all-gather.24.cloned.1.call-done = bf16[2048,512]{1,0:T(8,128)(2,1)} async-done(((bf16[512,512]{1,0:T(8,128)(2,1)}), bf16[2048,512]{1,0:T(8,128)(2,1)}) %all-gather.24.cloned.1.call-update) | async-done | bytes 2097168 | tf_op jit(solution)/shard_map/all_gather | solution.py:116
  427.0 34.9 %all-gather.18.cloned.1.call-done = bf16[1024,2048]{1,0:T(8,128)(2,1)} async-done(((bf16[256,2048]{1,0:T(8,128)(2,1)}), bf16[1024,2048]{1,0:T(8,128)(2,1)}) %all-gather.18.cloned.1.call-update) | async-done | bytes 4194320 | tf_op jit(solution)/shard_map/all_gather | solution.py:113
  461.9 5.2 convolution_convert_fusion.3
  470.3 73.9 %all-gather.22.cloned.1.call-done = bf16[2048,1024]{1,0:T(8,128)(2,1)} async-done(((bf16[512,1024]{1,0:T(8,128)(2,1)}), bf16[2048,1024]{1,0:T(8,128)(2,1)}) %all-gather.22.cloned.1.call-update) | async-done | bytes 4194320 | tf_op jit(solution)/shard_map/all_gather | solution.py:118
  544.2 7.9 convolution_convert_fusion.2
  552.6 2.6 copy.51
  555.2 34.8 %all-gather.20.cloned.1.call-done = bf16[2048,512]{1,0:T(8,128)(2,1)} async-done(((bf16[512,512]{1,0:T(8,128)(2,1)}), bf16[2048,512]{1,0:T(8,128)(2,1)}) %all-gather.20.cloned.1.call-update) | async-done | bytes 2097168 | tf_op jit(solution)/shard_map/all_gather | solution.py:117
  590.0 5.2 convolution_convert_fusion.4
  596.9 2.5 broadcast.96.clone2.1
  599.4 69.5 %while.30 = (s32[]{:T(128)}, f32[2,256,512]{2,1,0:T(8,128)S(1)}, f32[8,2,128,512]{3,2,0,1:T(8,128)}, f32[2]{0:T(128)S(1)}, f32[8,2,128,256]{3,2,0,1:T(8,128)}, /...) while((s32[]{:T(128)}, f32[2,256,512]{2,1,0:T(8,128)S(1)}, ...), condition=%wide.region_4.5_spmd.clone.clone.clone, body=%wide.region_3.4_spmd.clone.clone.clone.sunk | while | flops 1024885248 | bytes 8085164 | solution.py:49
  603.4 2.5 fusion.115
  605.8 2.2 convolution_add_fusion.4
  612.0 2.5 fusion.115
  614.5 2.2 convolution_add_fusion.4
  620.7 2.5 fusion.115
  623.2 2.2 convolution_add_fusion.4
  629.4 2.5 fusion.115
  631.9 2.2 convolution_add_fusion.4
  638.1 2.5 fusion.115
  640.6 2.2 convolution_add_fusion.4
  646.8 2.5 fusion.115
  649.3 2.2 convolution_add_fusion.4
  655.5 2.5 fusion.115
  658.0 2.2 convolution_add_fusion.4
  664.1 2.5 fusion.115
  666.7 2.2 convolution_add_fusion.4
  668.9 32.6 %rev.15 = f32[2,1024,512]{2,1,0:T(8,128)} reverse(f32[2,1024,512]{2,1,0:T(8,128)} %bitcast.191), dimensions={1} | reverse | bytes 8388608 | tf_op jit(solution)/shard_map/vmap(jit(_flip))/rev | solution.py:66
  701.5 16.8 %reverse.3 = f32[2,1024,256]{2,1,0:T(8,128)} reverse(f32[2,1024,256]{2,1,0:T(8,128)} %bitcast.199), dimensions={1} | reverse | bytes 4194304 | tf_op jit(solution)/shard_map/reverse
  718.3 3.1 broadcast_multiply_fusion
  721.4 10.3 %rev.14 = f32[2,1024,256]{2,1,0:T(8,128)} reverse(f32[2,1024,256]{2,1,0:T(8,128)S(1)} %bitcast.198), dimensions={1} | reverse | bytes 4194304 | tf_op jit(solution)/shard_map/vmap(jit(_flip))/rev | solution.py:65
  731.7 2.5 broadcast.96.clone2
  734.2 69.5 %while.31 = (s32[]{:T(128)}, f32[2,256,512]{2,1,0:T(8,128)S(1)}, f32[8,2,128,512]{3,2,0,1:T(8,128)}, f32[2]{0:T(128)S(1)}, f32[8,2,128,256]{3,2,0,1:T(8,128)}, /...) while((s32[]{:T(128)}, f32[2,256,512]{2,1,0:T(8,128)S(1)}, ...), condition=%wide.region_6.7_spmd.clone.clone.clone, body=%wide.region_5.6_spmd.clone.clone.clone.sunk | while | flops 1024885248 | bytes 8085164 | solution.py:49
  738.2 2.5 fusion.123
  740.7 2.2 convolution_add_fusion.5
  746.8 2.5 fusion.123
  749.3 2.2 convolution_add_fusion.5
  755.5 2.5 fusion.123
  758.1 2.2 convolution_add_fusion.5
  764.2 2.5 fusion.123
  766.7 2.2 convolution_add_fusion.5
  772.9 2.5 fusion.123
  775.4 2.2 convolution_add_fusion.5
  781.6 2.5 fusion.123
  784.1 2.2 convolution_add_fusion.5
  790.3 2.5 fusion.123
  792.8 2.2 convolution_add_fusion.5
  799.0 2.5 fusion.123
  801.5 2.2 convolution_add_fusion.5
  803.7 32.6 %rev.17 = f32[2,1024,512]{2,1,0:T(8,128)} reverse(f32[2,1024,512]{2,1,0:T(8,128)} %bitcast.195), dimensions={1} | reverse | bytes 8388608 | tf_op jit(solution)/shard_map/vmap(jit(_flip))/rev | solution.py:69
  836.4 4.0 fusion.65
  844.6 2.5 copy.24
  847.2 9.4 %convolution_convert_fusion.1 = bf16[1024,2048]{1,0:T(8,128)(2,1)} fusion(bf16[1024,1024]{0,1:T(8,128)(2,1)} %bitcast.204, bf16[1024,2048]{1,0:T(8,128)(2,1)} %all-gather.26.cloned.1.call-done), kind=kOutput, calls=%fused_computation.69 | convolution fusion | flops 4297064448 | bytes 10485760 | tf_op jit(solution)/shard_map/dot_general | solution.py:129
  856.6 43.6 %reduce-scatter.5.cloned.1.call-done = bf16[256,2048]{1,0:T(8,128)(2,1)} async-done(((bf16[1024,2048]{1,0:T(8,128)(2,1)}), bf16[256,2048]{1,0:T(8,128)(2,1)}) %reduce-scatter.5.cloned.1.call-update) | async-done | bytes 1048592 | tf_op jit(solution)/shard_map/reduce_scatter | solution.py:134
  900.2 2.7 fusion.58
  (142 shorter events, 79.3 us)
Async XLA Ops:
  6.5 41.4 %all-gather.10.cloned.1.call-start = ((), (), s32[]{:S(2)}) async-start(), calls=%async_computation.2 | async-start | bytes 5242880 | tf_op jit(solution)/shard_map/all_gather | solution.py:86
  10.6 128.3 %all-gather.12.cloned.1.call-start = ((), (), s32[]{:S(2)}) async-start(), calls=%async_computation.3 | async-start | bytes 5898240 | tf_op jit(solution)/shard_map/all_gather | solution.py:89
  11.3 217.0 %all-gather.14.cloned.1.call-start = ((), (), s32[]{:S(2)}) async-start(), calls=%async_computation.4 | async-start | bytes 5898240 | tf_op jit(solution)/shard_map/all_gather | solution.py:94
  12.1 305.5 %all-gather.16.cloned.1.call-start = ((), (), s32[]{:S(2)}) async-start(), calls=%async_computation.5 | async-start | bytes 5898240 | tf_op jit(solution)/shard_map/all_gather | solution.py:100
  12.7 367.2 %reduce-scatter.3.cloned.1.call-start = ((), (), s32[]{:S(2)}) async-start(), calls=%async_computation.6 | async-start | bytes 5242880 | tf_op jit(solution)/shard_map/reduce_scatter | solution.py:103
  336.7 43.2 %copy-start.2 = (bf16[256,2048]{1,0:T(8,128)(2,1)S(1)}, bf16[256,2048]{1,0:T(8,128)(2,1)}, u32[]{:S(2)}) copy-start(bf16[256,2048]{1,0:T(8,128)(2,1)} %param.16) | copy-start | bytes 3145732
  336.7 44.9 %copy-start.6 = (f32[2048]{0:T(1024)S(1)}, f32[2048]{0:T(1024)}, u32[]{:S(2)}) copy-start(f32[2048]{0:T(1024)} %param.18) | copy-start | bytes 24580
  336.8 90.2 %all-gather.24.cloned.1.call-start = ((), (), s32[]{:S(2)}) async-start(), calls=%async_computation.10 | async-start | bytes 2621440 | tf_op jit(solution)/shard_map/all_gather | solution.py:116
  337.4 49.4 %copy-start.8 = (f32[2,2]{1,0:T(2,128)S(1)}, f32[2,2]{1,0:T(2,128)}, u32[]{:S(2)}) copy-start(f32[2,2]{1,0:T(2,128)} %param.27) | copy-start | bytes 52
  337.4 49.4 %copy-start.7 = (f32[1024]{0:T(1024)S(1)}, f32[1024]{0:T(1024)}, u32[]{:S(2)}) copy-start(f32[1024]{0:T(1024)} %param.25) | copy-start | bytes 12292
  337.4 124.5 %all-gather.18.cloned.1.call-start = ((), (), s32[]{:S(2)}) async-start(), calls=%async_computation.7 | async-start | bytes 5242880 | tf_op jit(solution)/shard_map/all_gather | solution.py:113
  384.3 159.9 %all-gather.22.cloned.1.call-start = ((), (), s32[]{:S(2)}) async-start(), calls=%async_computation.9 | async-start | bytes 5242880 | tf_op jit(solution)/shard_map/all_gather | solution.py:118
  385.1 204.9 %all-gather.20.cloned.1.call-start = ((), (), s32[]{:S(2)}) async-start(), calls=%async_computation.8 | async-start | bytes 2621440 | tf_op jit(solution)/shard_map/all_gather | solution.py:117
  385.8 461.4 %all-gather.26.cloned.1.call-start = ((), (), s32[]{:S(2)}) async-start(), calls=%async_computation.11 | async-start | bytes 5242880 | tf_op jit(solution)/shard_map/all_gather | solution.py:131
  386.4 513.8 %reduce-scatter.5.cloned.1.call-start = ((), (), s32[]{:S(2)}) async-start(), calls=%async_computation.12 | async-start | bytes 5242880 | tf_op jit(solution)/shard_map/reduce_scatter | solution.py:134
  701.5 19.9 %copy-start.4 = (f32[8,2,128,256]{3,2,0,1:T(8,128)S(1)}, f32[8,2,128,256]{3,2,0,1:T(8,128)}, u32[]{:S(2)}) copy-start(f32[8,2,128,256]{3,2,0,1:T(8,128)} %get-tuple-element.681) | copy-start | bytes 6291460
  836.4 4.6 copy-start
  836.4 5.9 copy-start.1
  856.6 43.6 %copy-start.3 = (bf16[256,2048]{1,0:T(8,128)(2,1)S(1)}, bf16[256,2048]{1,0:T(8,128)(2,1)}, u32[]{:S(2)}) copy-start(bf16[256,2048]{1,0:T(8,128)(2,1)} %param.16) | copy-start | bytes 3145732
  856.6 43.6 %copy-start.5 = (bf16[256,2048]{1,0:T(8,128)(2,1)S(1)}, bf16[256,2048]{1,0:T(8,128)(2,1)}, u32[]{:S(2)}) copy-start(bf16[256,2048]{1,0:T(8,128)(2,1)} %reduce-scatter.3.cloned.1.call-done) | copy-start | bytes 3145732
Sparse Core Ops, SparseCore 0:
  10.7 37.1 all-gather.9
  49.5 89.3 all-gather.11
  140.5 87.7 all-gather.13
  229.7 87.7 all-gather.15
  336.9 42.9 reduce-scatter.2
  381.3 45.6 all-gather.23
  428.6 33.2 all-gather.17
  463.4 80.7 all-gather.21
  545.8 44.1 all-gather.19
  591.4 79.5 all-gather.25
  856.7 43.4 reduce-scatter.4
where the time goes:
time: 918 us; the launch traced here: 909 us
  waiting for transfers between devices  569 us (62%)
  matrix products  176 us (19%)
  local copies, waits for them, and re-layouts  125 us (14%)
  other arithmetic  24.4 us (3%)
  between operations  13.4 us (1%)
    all_gather x1, waiting for transfers between devices, feed_half(): lax.all_gather(gate_weight, 'fs', axis=0, tiled=True)  91 us
    all_gather x1, waiting for transfers between devices, feed_half(): lax.all_gather(down_weight, 'fs', axis=1, tiled=True)  89.3 us
    all_gather x1, waiting for transfers between devices, feed_half(): lax.all_gather(up_weight, 'fs', axis=0, tiled=True)  79.2 us
    all_gather x1, waiting for transfers between devices, mix_tokens(): lax.all_gather(value_weight, 'fs', axis=0, tiled=True)  73.9 us
    reduce_scatter x1, waiting for transfers between devices, mix_tokens(): lax.psum_scatter(partial_out.astype(jnp.bfloat16), 'tp', scatter_dimensio...  43.6 us
    reduce_scatter x1, waiting for transfers between devices, feed_half(): lax.psum_scatter(partial_out.astype(jnp.bfloat16), 'tp', scatter_dimensio...  42.5 us
    all_gather x1, waiting for transfers between devices, mix_tokens(): lax.all_gather(query_weight, 'fs', axis=0, tiled=True)  40.2 us
    dot_general x16, matrix products, advance(): jnp.dot(query_block, memory, precision=highest) * enter_decay[:, None]  40 us
  transfers between devices with their start and end apart: 11, of which 10 were waited for; matrix products, arithmetic and copies ran while one was open for 32% of the time, Pallas kernels for 0%

commit v1 on v0

v1 whole, which is shorter than its diff:
```python
import functools

import jax
import jax.numpy as jnp
from jax import lax
from jax.experimental import pallas as pl
from jax.experimental.pallas import tpu as pltpu
from jax.sharding import PartitionSpec as P

DK = 256
DV = 512
EPS = 1e-06


def norm_rows(values, gain):
    widened = values.astype(jnp.float32)
    factor = lax.rsqrt(jnp.mean(widened * widened, axis=-1, keepdims=True) + EPS)
    return (widened * factor * gain).astype(jnp.bfloat16)


def matmul(left, right):
    return jnp.dot(left, right, preferred_element_type=jnp.float32)


def chip_shift(value, chips, shift):
    pairs = [
        (((chip + shift) % chips) * 2 + core, chip * 2 + core)
        for chip in range(chips)
        for core in range(2)
    ]
    return lax.ppermute(value, "tp", pairs)


def core_swap(value, chips):
    return lax.ppermute(value, "tp", [(at, at ^ 1) for at in range(2 * chips)])


def chunk_ids(chips):
    at = lax.axis_index("tp")
    chip, core = at // 2, at % 2
    ahead = (chip + jnp.arange(chips, dtype=jnp.int32)) % chips
    return jnp.concatenate([ahead * 2 + core, ahead * 2 + 1 - core]).astype(jnp.int32)


def gather_rows(own, chips):
    same = [own] + [chip_shift(own, chips, shift) for shift in range(1, chips)]
    other = [core_swap(piece, chips) for piece in same]
    return jnp.concatenate(same + other, axis=0)


def scatter_sum(same_core, other_core, chips):
    swapped = core_swap(other_core, chips)
    summed = same_core.astype(jnp.float32) + swapped.astype(jnp.float32)
    rows = summed.shape[0] // chips
    total = summed[:rows]
    for shift in range(1, chips):
        piece = summed[shift * rows : (shift + 1) * rows].astype(jnp.bfloat16)
        total = total + chip_shift(piece, chips, chips - shift).astype(jnp.float32)
    return total


def local_order(values, n_fs, halve):
    if not halve:
        return values
    group, at = lax.axis_index("grp"), lax.axis_index("fs")
    blocks = values.reshape(values.shape[0], n_fs, 2, -1)
    mine = lax.dynamic_index_in_dim(blocks, group, 2, keepdims=False)
    other = lax.dynamic_index_in_dim(blocks, 1 - group, 2, keepdims=False)
    other = lax.dynamic_slice_in_dim(jnp.concatenate([other, other], axis=1), at, n_fs, 1)
    return jnp.concatenate([mine, other], axis=1).reshape(values.shape)


def whole_order(values, n_fs, halve):
    if not halve:
        return values
    group, at = lax.axis_index("grp"), lax.axis_index("fs")
    blocks = values.reshape(values.shape[0], 2, n_fs, -1)
    mine, other = blocks[:, 0], blocks[:, 1]
    other = lax.dynamic_slice_in_dim(
        jnp.concatenate([other, other], axis=1), (n_fs - at) % n_fs, n_fs, 1
    )
    first = jnp.where(group == 0, mine, other)
    second = jnp.where(group == 0, other, mine)
    return jnp.stack([first, second], axis=2).reshape(values.shape)


def fetch(weight, axis, halve, n_fs, name):
    if not halve:
        return [lax.all_gather(weight, "fs", axis=0, tiled=False)]
    group, at = lax.axis_index("grp"), lax.axis_index("fs")
    half = weight.shape[axis] // 2
    mine = lax.dynamic_slice_in_dim(weight, group * half, half, axis)
    other = lax.dynamic_slice_in_dim(weight, (1 - group) * half, half, axis)
    gathered = lax.all_gather(mine, "fs", axis=0, tiled=False)
    if int(name[1:]) % 2:
        rows = gathered.shape[1]
        lines = flat(gathered)
        lines = jnp.concatenate([lines, lines[: (n_fs - 2) * rows]], axis=0)
        start = (at + 1) % n_fs * rows
        sent = lax.dynamic_slice_in_dim(lines, start, (n_fs - 1) * rows, 0)
    else:
        sent = jnp.stack(
            [
                lax.dynamic_index_in_dim(gathered, (at + step) % n_fs, 0, keepdims=False)
                for step in range(1, n_fs)
            ]
        )
    received = lax.ppermute(sent, "grp", [(0, 1), (1, 0)])
    received = received.reshape(n_fs - 1, *other.shape)
    return [gathered, jnp.concatenate([other[None], received], axis=0)]


def flat(stacked):
    return stacked.reshape(-1, stacked.shape[-1])


def split_matmul(rows, parts):
    total, at = None, 0
    for part in map(flat, parts):
        piece = matmul(rows[:, at : at + part.shape[0]], part)
        total, at = piece if total is None else total + piece, at + part.shape[0]
    return total


def project_body(left, right, out):
    out[...] = jnp.dot(left[...], right[0], preferred_element_type=jnp.float32).astype(jnp.bfloat16)


def project(left, right, first_row, rows):
    blocks, depth, width = right.shape
    base = first_row // rows
    return pl.pallas_call(
        project_body,
        grid=(blocks,),
        in_specs=[
            pl.BlockSpec((rows, depth), lambda f: (base, 0)),
            pl.BlockSpec((1, depth, width), lambda f: (f, 0, 0)),
        ],
        out_specs=pl.BlockSpec((rows, width), lambda f: (0, f)),
        out_shape=jax.ShapeDtypeStruct((rows, blocks * width), jnp.bfloat16),
        cost_estimate=pl.CostEstimate(
            flops=2 * rows * blocks * width * depth,
            bytes_accessed=2 * (rows * depth + (rows + depth) * blocks * width),
            transcendentals=0,
        ),
    )(left, right)


def retain_body(chunks, rows, ids, rates, queries, keys, values, gain, out):
    head, here = pl.program_id(0), pl.program_id(1)
    forward, backward = rates[0, head], rates[1, head]
    row = lax.broadcasted_iota(jnp.int32, (rows, rows), 0)
    column = lax.broadcasted_iota(jnp.int32, (rows, rows), 1)
    apart = row - column
    query = queries[...]
    total = jnp.zeros((rows, DV), jnp.float32)
    for at in range(chunks):
        part = pl.ds(at * rows, rows)
        scores = lax.dot_general(
            query, keys[part, :], (((1,), (1,)), ((), ())), preferred_element_type=jnp.float32
        )
        steps = apart + (ids[here] - ids[at]) * rows
        distance = steps.astype(jnp.float32)
        decay = jnp.exp(jnp.where(steps >= 0, forward * distance, -backward * distance))
        decay = jnp.where(steps == 0, 2.0, decay) * DK**-0.5
        total = total + jnp.dot(
            (scores * decay).astype(jnp.bfloat16), values[part, :], preferred_element_type=jnp.float32
        )
    centered = total - jnp.mean(total, axis=-1, keepdims=True)
    variance = jnp.mean(centered * centered, axis=-1, keepdims=True)
    out[...] = (centered * lax.rsqrt(variance + EPS) * gain[0]).astype(jnp.bfloat16)


def retain(query_keys, values, gain, rates, ids):
    length, heads, chunks = values.shape[0], rates.shape[1], ids.shape[0]
    rows = length // chunks
    scalars = pl.BlockSpec(memory_space=pltpu.SMEM)
    return pl.pallas_call(
        functools.partial(retain_body, chunks, rows),
        grid=(heads, chunks),
        in_specs=[
            scalars,
            scalars,
            pl.BlockSpec((rows, DK), lambda h, r: (r, h)),
            pl.BlockSpec((length, DK), lambda h, r: (0, heads + h)),
            pl.BlockSpec((length, DV), lambda h, r: (0, h)),
            pl.BlockSpec((1, 1, DV), lambda h, r: (h, 0, 0)),
        ],
        out_specs=pl.BlockSpec((rows, DV), lambda h, r: (r, h)),
        out_shape=jax.ShapeDtypeStruct((length, heads * DV), jnp.bfloat16),
        cost_estimate=pl.CostEstimate(
            flops=2 * heads * length * length * (DK + DV),
            bytes_accessed=4 * heads * length * (DK + DV),
            transcendentals=heads * length * length,
        ),
        name="retain",
    )(ids, rates, query_keys, query_keys, values, gain.reshape(heads, 1, DV))


def project_sum(left, parts, chips):
    half = left.shape[0] // 2
    sums = []
    for part in parts:
        other_core = project(left, part, half, half)
        same_core = project(left, part, 0, half)
        sums.append(scatter_sum(same_core, other_core, chips))
    return jnp.concatenate(sums, axis=1)


def shards(
    n_grp,
    n_fs,
    n_tp,
    tokens,
    first_gain,
    mixer_gain,
    gate_weight,
    up_weight,
    down_weight,
    query_weight,
    key_weight,
    value_weight,
    head_gain,
    out_weight,
    log_decay,
):
    chips = n_tp // 2
    halve = n_grp == 2 and down_weight.shape[1] % 256 == 0
    gates = fetch(gate_weight, 0, halve, n_fs, "w0")
    ups = fetch(up_weight, 0, halve, n_fs, "w1")
    downs = fetch(down_weight, 1, halve, n_fs, "w2")
    both = jnp.concatenate([query_weight, key_weight], axis=1)
    query_keys = fetch(both, 0, halve, n_fs, "w3")
    values = fetch(value_weight, 0, halve, n_fs, "w4")
    outs = fetch(out_weight, 1, halve, n_fs, "w5")

    here = local_order(tokens, n_fs, halve)
    gains = local_order(jnp.stack([first_gain, mixer_gain]), n_fs, halve)
    rows = gather_rows(norm_rows(here, gains[0]), chips)
    hidden = jax.nn.silu(split_matmul(rows, gates)) * split_matmul(rows, ups)
    branch = project_sum(hidden.astype(jnp.bfloat16), downs, chips)
    after_first = (here.astype(jnp.float32) + 0.5 * branch).astype(jnp.bfloat16)

    rows = gather_rows(norm_rows(after_first, gains[1]), chips)
    projected = split_matmul(rows, query_keys).astype(jnp.bfloat16)
    retained = retain(
        projected,
        split_matmul(rows, values).astype(jnp.bfloat16),
        head_gain,
        log_decay,
        chunk_ids(chips),
    )
    branch = project_sum(retained, outs, chips)
    updated = (after_first.astype(jnp.float32) + branch).astype(jnp.bfloat16)
    return whole_order(updated, n_fs, halve)


def solution(mesh):
    placed = (
        P(("grp", "fs", "tp"), None),
        P(),
        P(),
        P("fs", "tp"),
        P("fs", "tp"),
        P("tp", "fs"),
        P("fs", "tp"),
        P("fs", "tp"),
        P("fs", "tp"),
        P("tp"),
        P("tp", "fs"),
        P(None, "tp"),
    )
    sizes = mesh.shape
    body = functools.partial(shards, sizes["grp"], sizes["fs"], sizes["tp"])
    return jax.shard_map(
        body, mesh=mesh, in_specs=placed, out_specs=P(("grp", "fs", "tp"), None), check_vma=False
    )
```

time: 918 us -> 432 us (0.47)
  waiting for transfers between devices: 569 us -> 225 us
  matrix products: 176 us -> 25.4 us
  local copies, waits for them, and re-layouts: 125 us -> 38.7 us
  Pallas kernels: 0 us -> 52.4 us
  other arithmetic: 24.4 us -> 53.7 us
  starting transfers between devices: 0.57 us -> 17.6 us
    all_gather x9 -> x6, waiting for transfers between devices: 478 us -> 120 us  [fetch(): gathered = lax.all_gather(mine, 'fs', axis=0, tiled=False)]
    dot_general x70 -> x8, matrix products: 176 us -> 25.4 us  [matmul(): return jnp.dot(left, right, preferred_element_type=jnp.float32)]
    ppermute x0 -> x20, waiting for transfers between devices: none -> 104 us  [the longest x6 64.8 us: chip_shift(): return lax.ppermute(value, 'tp', pairs)]
    reduce_scatter x2 -> x0, waiting for transfers between devices: 86.1 us -> none  [the longest x1 43.6 us: mix_tokens(): lax.psum_scatter(partial_out.astype(jnp.bfloat16), 'tp', scatter_dimensio...]
    rev x3 -> x0, local copies, waits for them, and re-layouts: 75.6 us -> none  [the longest x1 32.6 us: retain_both(): jnp.flip(value_rows, axis=0)]
    pallas_call x0 -> x9, Pallas kernels: none -> 52.4 us  [the longest x8 40.5 us: project(): pl.pallas_call(project_body, grid=(blocks,), in_specs=[pl.BlockSpec((rows...]
    concatenate x0 -> x14, other arithmetic: none -> 32.5 us  [the longest x6 12.8 us: fetch(): return [gathered, jnp.concatenate([other[None], received], axis=0)]]
    another operation x3 -> x4, local copies, waits for them, and re-layouts: 21.8 us -> 0.55 us  [the longest x1 0.52 us: whole_order(): return jnp.stack([first, second], axis=2).reshape(values.shape)]
  transfers between devices with their start and end apart: 11 -> 26, of which waited for: 10 -> 12; matrix products, arithmetic and copies ran while one was open for 32% -> 24% of each run, Pallas kernels for 0% -> 12%
where the time goes in v1:
time: 432 us; the launch traced here: 427 us
  waiting for transfers between devices  225 us (52%)
  other arithmetic  53.7 us (12%)
  Pallas kernels  52.4 us (12%)
  local copies, waits for them, and re-layouts  38.7 us (9%)
  matrix products  25.4 us (6%)
  starting transfers between devices  17.6 us (4%)
  between operations  14.5 us (3%)
    all_gather x6, waiting for transfers between devices, fetch(): gathered = lax.all_gather(mine, 'fs', axis=0, tiled=False)  120 us
    ppermute x6, waiting for transfers between devices, chip_shift(): return lax.ppermute(value, 'tp', pairs)  64.8 us
    pallas_call x8, Pallas kernels, project(): pl.pallas_call(project_body, grid=(blocks,), in_specs=[pl.BlockSpec((rows...  40.5 us
    ppermute x6, waiting for transfers between devices, fetch(): received = lax.ppermute(sent, 'grp', [(0, 1), (1, 0)])  39.2 us
    dot_general x8, matrix products, matmul(): return jnp.dot(left, right, preferred_element_type=jnp.float32)  25.4 us
    concatenate x10, local copies, waits for them, and re-layouts, project_sum(): return jnp.concatenate(sums, axis=1)  14.5 us
    concatenate x6, other arithmetic, fetch(): return [gathered, jnp.concatenate([other[None], received], axis=0)]  12.8 us
    concatenate x3, other arithmetic, fetch(): lines = jnp.concatenate([lines, lines[:(n_fs - 2) * rows]], axis=0)  12.4 us
  transfers between devices with their start and end apart: 26, of which 12 were waited for; matrix products, arithmetic and copies ran while one was open for 24% of the time, Pallas kernels for 12%

profile of v1, /device:TPU:0, one launch (start us, length us, event | category | flops | bytes accessed | tf_op | source)
XLA Modules:
  0.0 426.9 jit_solution(17431075947663397431)
XLA Ops:
  6.5 2.5 dynamic-slice_bitcast_fusion.2
  14.9 1.6 fusion.31
  17.4 3.0 collective-permute-start
  20.4 23.3 %collective-permute-done = bf16[256,2048]{1,0:T(8,128)(2,1)} collective-permute-done((bf16[256,2048]{1,0:T(8,128)(2,1)S(1)}, bf16[256,2048]{1,0:T(8,128)(2,1)}, u32[]{:S(2)}, u32[]{:S(2)}) %collective-permute-start) | collective-permute-done | bytes 1048608 | tf_op jit(solution)/shard_map/ppermute | solution.py:31
  44.9 17.0 %all-gather.13.cloned.1.call-done = bf16[1024,1152]{1,0:T(8,128)(2,1)} async-done(((bf16[256,1152]{1,0:T(8,128)(2,1)}), bf16[1024,1152]{1,0:T(8,128)(2,1)}) %all-gather.13.cloned.1.call-update) | async-done | bytes 2359312 | tf_op jit(solution)/shard_map/all_gather | solution.py:94
  61.9 1.6 constant_dynamic-slice_fusion.13
  63.5 1.5 pad_maximum_fusion.8
  64.9 1.5 collective-permute-start.3
  66.4 3.9 pad_maximum_fusion
  70.3 41.9 %all-gather.15.cloned.1.call-done = bf16[1024,1152]{1,0:T(8,128)(2,1)} async-done(((bf16[256,1152]{1,0:T(8,128)(2,1)}), bf16[1024,1152]{1,0:T(8,128)(2,1)}) %all-gather.15.cloned.1.call-update) | async-done | bytes 2359312 | tf_op jit(solution)/shard_map/all_gather | solution.py:94
  113.5 4.2 fusion.20
  117.8 1.5 collective-permute-start.4
  119.2 43.4 %all-gather.17.cloned.1.call-done = bf16[4608,256]{1,0:T(8,128)(2,1)} async-done(((bf16[1152,256]{1,0:T(8,128)(2,1)}), bf16[4608,256]{1,0:T(8,128)(2,1)}) %all-gather.17.cloned.1.call-update) | async-done | bytes 2359312 | tf_op jit(solution)/shard_map/all_gather | solution.py:94
  162.6 1.7 constant_dynamic-slice_fusion.8
  164.3 1.5 pad_maximum_fusion.9
  165.8 1.5 collective-permute-start.7
  167.3 2.9 fusion.18
  170.2 1.8 pad_maximum_fusion.2
  171.9 2.9 fusion.15
  174.8 1.7 pad_maximum_fusion.3
  176.6 2.9 fusion.13
  179.5 4.7 %multiply_convert_fusion.left = bf16[1024,1152]{1,0:T(8,128)(2,1)} fusion(f32[1024,1152]{1,0:T(8,128)S(1)} %fusion.13, f32[1024,1152]{1,0:T(8,128)S(1)} %fusion.18, f32[1024,1152]{1,0:T(8,128)S(1)} %fusion.15, bf16[1024,1152]{1,0:T(8,128)(2,1)S(1)} %copy-done.15, bf16[1024,2048]{1,0:T(8,128)(2,1)S(1)} %copy-done.20), kind=kOutput, calls=%fused_computation | convolution fusion | flops 2425356288 | bytes 20971520 | tf_op jit(solution)/shard_map/dot_general | solution.py:22
  184.2 5.1 %shard_map.119 = bf16[512,1024]{1,0:T(8,128)(2,1)} custom-call(bf16[1024,1152]{1,0:T(8,128)(2,1)} %multiply_convert_fusion.left, bf16[4,1152,256]{2,1,0:T(8,128)(2,1)} %bitcast.75), custom_call_target="tpu_custom_call" | custom-call | flops 1207959552 | bytes 4587520 | tf_op jit(solution)/shard_map/pallas_call | solution.py:132
  189.3 17.0 %collective-permute-done.7 = bf16[3,1152,256]{2,1,0:T(8,128)(2,1)} collective-permute-done((bf16[3,1152,256]{2,1,0:T(8,128)(2,1)}, bf16[3,1152,256]{2,1,0:T(8,128)(2,1)}, u32[]{:S(2)}, u32[]{:S(2)}) %collective-permute-start.7) | collective-permute-done | bytes 1769504 | tf_op jit(solution)/shard_map/ppermute | solution.py:108
  206.3 3.2 pad_maximum_fusion.4.right
  209.4 5.0 %shard_map.121 = bf16[512,1024]{1,0:T(8,128)(2,1)} custom-call(bf16[1024,1152]{1,0:T(8,128)(2,1)} %multiply_convert_fusion.left, bf16[4,1152,256]{2,1,0:T(8,128)(2,1)} %pad_maximum_fusion.4.right), custom_call_target="tpu_custom_call" | custom-call | flops 1207959552 | bytes 4587520 | tf_op jit(solution)/shard_map/pallas_call | solution.py:132
  214.4 5.7 %shard_map.118 = bf16[512,1024]{1,0:T(8,128)(2,1)} custom-call(bf16[1024,1152]{1,0:T(8,128)(2,1)} %multiply_convert_fusion.left, bf16[4,1152,256]{2,1,0:T(8,128)(2,1)} %bitcast.76), custom_call_target="tpu_custom_call" | custom-call | flops 1207959552 | bytes 4587520 | tf_op jit(solution)/shard_map/pallas_call | solution.py:132
  220.1 5.2 %shard_map.120 = bf16[512,1024]{1,0:T(8,128)(2,1)} custom-call(bf16[1024,1152]{1,0:T(8,128)(2,1)} %multiply_convert_fusion.left, bf16[4,1152,256]{2,1,0:T(8,128)(2,1)} %pad_maximum_fusion.4.right), custom_call_target="tpu_custom_call" | custom-call | flops 1207959552 | bytes 4587520 | tf_op jit(solution)/shard_map/pallas_call | solution.py:132
  225.3 1.7 convert_add_fusion.3
  227.1 1.5 collective-permute-start.6
  228.6 1.6 convert_add_fusion.2
  233.9 8.2 %collective-permute-done.6 = bf16[256,1024]{1,0:T(8,128)(2,1)} collective-permute-done((bf16[256,1024]{1,0:T(8,128)(2,1)S(1)}, bf16[256,1024]{1,0:T(8,128)(2,1)}, u32[]{:S(2)}, u32[]{:S(2)}) %collective-permute-start.6) | collective-permute-done | bytes 524320 | tf_op jit(solution)/shard_map/ppermute | solution.py:31
  243.4 9.5 %collective-permute-done.9 = bf16[256,1024]{1,0:T(8,128)(2,1)} collective-permute-done((bf16[256,1024]{1,0:T(8,128)(2,1)}, bf16[256,1024]{1,0:T(8,128)(2,1)}, u32[]{:S(2)}, u32[]{:S(2)}) %collective-permute-start.9) | collective-permute-done | bytes 524320 | tf_op jit(solution)/shard_map/ppermute | solution.py:31
  257.9 2.9 fusion.22
  260.8 1.5 collective-permute-start.13
  262.3 1.6 constant_dynamic-slice_fusion.3
  265.8 15.7 %collective-permute-done.10 = bf16[256,2048]{1,0:T(8,128)(2,1)} collective-permute-done((bf16[256,2048]{1,0:T(8,128)(2,1)}, bf16[256,2048]{1,0:T(8,128)(2,1)}, u32[]{:S(2)}, u32[]{:S(2)}) %collective-permute-start.10) | collective-permute-done | bytes 1048608 | tf_op jit(solution)/shard_map/ppermute | solution.py:31
  282.2 18.1 %all-gather.23.cloned.1.call-done = bf16[4096,256]{1,0:T(8,128)(2,1)} async-done(((bf16[1024,256]{1,0:T(8,128)(2,1)}), bf16[4096,256]{1,0:T(8,128)(2,1)}) %all-gather.23.cloned.1.call-update) | async-done | bytes 2097168 | tf_op jit(solution)/shard_map/all_gather | solution.py:94
  301.5 5.2 %fusion.21 = bf16[3072,256]{1,0:T(8,128)(2,1)} fusion(s32[]{:T(128)S(6)} %select_n.137, bf16[4096,256]{1,0:T(8,128)(2,1)} %all-gather.23.cloned.1.call-done, bf16[2048,256]{1,0:T(8,128)(2,1)S(1)} %slice-done), kind=kLoop, calls=%fused_computation.52 | loop fusion | flops 3145728 | bytes 4718596 | tf_op jit(solution)/shard_map/concatenate | solution.py:98
  306.8 1.5 collective-permute-start.17
  308.2 1.6 pad_maximum_fusion.5
  309.9 22.2 %collective-permute-done.14 = bf16[3,256,1024]{2,1,0:T(8,128)(2,1)} collective-permute-done((bf16[3,256,1024]{2,1,0:T(8,128)(2,1)}, bf16[3,256,1024]{2,1,0:T(8,128)(2,1)}, u32[]{:S(2)}, u32[]{:S(2)}) %collective-permute-start.14) | collective-permute-done | bytes 1572896 | tf_op jit(solution)/shard_map/ppermute | solution.py:108
  332.1 1.6 pad_maximum_fusion.6
  333.7 2.6 pad_maximum_fusion.1
  336.3 2.3 fusion.7
  338.6 3.7 add_convert_fusion.values
  342.3 2.3 fusion.9
  344.6 3.7 add_convert_fusion.1.queries.keys
  348.4 11.9 %retain.1.left = bf16[1024,1024]{1,0:T(8,128)(2,1)} custom-call(s32[4]{0:T(128)} %pad_add_fusion.ids, f32[2,2]{1,0:T(2,128)} %rates.1, bf16[1024,1024]{1,0:T(8,128)(2,1)} %add_convert_fusion.1.queries.keys, bf16[1024,1024]{1,0:T(8,128)(2,1)} %add_convert_fusion.1.queries.keys, bf16[1024,1024]{1,0:T(8,128)(2,1)} %add_convert_fusion.values, f32[2,1,512]{2,1,0:T(1,128)} %bitcast.96), custom_call_target="tpu_custom_call" | custom-call | flops 3221225472 | bytes 6291456 | tf_op jit(solution)/shard_map/retain/pallas_call | solution.py:178
  360.3 4.9 %shard_map.123 = bf16[512,1024]{1,0:T(8,128)(2,1)} custom-call(bf16[1024,1024]{1,0:T(8,128)(2,1)} %retain.1.left, bf16[4,1024,256]{2,1,0:T(8,128)(2,1)} %bitcast.70), custom_call_target="tpu_custom_call" | custom-call | flops 1073741824 | bytes 4194304 | tf_op jit(solution)/shard_map/pallas_call | solution.py:132
  365.1 2.9 pad_maximum_fusion.7.right
  368.1 4.7 %shard_map.125 = bf16[512,1024]{1,0:T(8,128)(2,1)} custom-call(bf16[1024,1024]{1,0:T(8,128)(2,1)} %retain.1.left, bf16[4,1024,256]{2,1,0:T(8,128)(2,1)} %pad_maximum_fusion.7.right), custom_call_target="tpu_custom_call" | custom-call | flops 1073741824 | bytes 4194304 | tf_op jit(solution)/shard_map/pallas_call | solution.py:132
  373.3 4.8 %shard_map.122 = bf16[512,1024]{1,0:T(8,128)(2,1)} custom-call(bf16[1024,1024]{1,0:T(8,128)(2,1)} %retain.1.left, bf16[4,1024,256]{2,1,0:T(8,128)(2,1)} %bitcast.71), custom_call_target="tpu_custom_call" | custom-call | flops 1073741824 | bytes 4194304 | tf_op jit(solution)/shard_map/pallas_call | solution.py:132
  378.1 5.1 %shard_map.124 = bf16[512,1024]{1,0:T(8,128)(2,1)} custom-call(bf16[1024,1024]{1,0:T(8,128)(2,1)} %retain.1.left, bf16[4,1024,256]{2,1,0:T(8,128)(2,1)} %pad_maximum_fusion.7.right), custom_call_target="tpu_custom_call" | custom-call | flops 1073741824 | bytes 4194304 | tf_op jit(solution)/shard_map/pallas_call | solution.py:132
  385.6 1.6 convert_add_fusion
  392.0 2.5 copy.26
  394.6 5.3 %collective-permute-done.16 = bf16[256,1024]{1,0:T(8,128)(2,1)} collective-permute-done((bf16[256,1024]{1,0:T(8,128)(2,1)}, bf16[256,1024]{1,0:T(8,128)(2,1)}, u32[]{:S(2)}, u32[]{:S(2)}) %collective-permute-start.16) | collective-permute-done | bytes 524320 | tf_op jit(solution)/shard_map/ppermute | solution.py:31
  399.9 2.1 slice_add_fusion.1
  402.0 2.9 concatenate.102
  404.9 2.4 copy.29
  407.3 2.9 collective-permute-done.19
  410.1 2.1 slice_add_fusion
  412.3 2.9 concatenate.105
  415.1 1.6 copy.30
  (179 shorter events, 33.4 us)
Async XLA Ops:
  6.5 2.6 copy-start.33
  6.5 55.4 %all-gather.13.cloned.1.call-start = ((), (), s32[]{:S(2)}) async-start(), calls=%async_computation | async-start | bytes 2949120 | tf_op jit(solution)/shard_map/all_gather | solution.py:94
  9.0 1.6 copy-start.34
  9.0 103.2 %all-gather.15.cloned.1.call-start = ((), (), s32[]{:S(2)}) async-start(), calls=%async_computation.1 | async-start | bytes 2949120 | tf_op jit(solution)/shard_map/all_gather | solution.py:94
  10.2 1.7 copy-start.38
  10.2 1.7 copy-start.39
  10.3 152.3 %all-gather.17.cloned.1.call-start = ((), (), s32[]{:S(2)}) async-start(), calls=%async_computation.2 | async-start | bytes 2949120 | tf_op jit(solution)/shard_map/all_gather | solution.py:94
  11.8 222.0 %all-gather.19.cloned.1.call-start = ((), (), s32[]{:S(2)}) async-start(), calls=%async_computation.3 | async-start | bytes 2621440 | tf_op jit(solution)/shard_map/all_gather | solution.py:94
  12.0 1.6 copy-start.35
  13.2 249.1 %all-gather.21.cloned.1.call-start = ((), (), s32[]{:S(2)}) async-start(), calls=%async_computation.4 | async-start | bytes 2621440 | tf_op jit(solution)/shard_map/all_gather | solution.py:94
  14.6 2.1 copy-start.3
  14.9 1.9 copy-start.5
  16.8 26.9 %copy-start.36 = (bf16[512,1024]{1,0:T(8,128)(2,1)S(1)}, bf16[512,1024]{1,0:T(8,128)(2,1)}, u32[]{:S(2)}) copy-start(bf16[512,1024]{1,0:T(8,128)(2,1)} %param.20) | copy-start | bytes 3145732
  17.4 26.3 %collective-permute-start = (bf16[256,2048]{1,0:T(8,128)(2,1)S(1)}, bf16[256,2048]{1,0:T(8,128)(2,1)}, u32[]{:S(2)}, u32[]{:S(2)}) collective-permute-start(bf16[256,2048]{1,0:T(8,128)(2,1)S(1)} %multiply_convert_fusion.2), channel_id=1, source_target_pairs={{2,0},{3,1},{0,2},{1,3},{6,4},{7,5},{4,6},{5,7},{10,8},{11,9},{8,1... | collective-permute-start | bytes 3145736 | tf_op jit(solution)/shard_map/ppermute | solution.py:31
  20.4 46.0 %collective-permute-start.1 = (bf16[256,2048]{1,0:T(8,128)(2,1)S(1)}, bf16[256,2048]{1,0:T(8,128)(2,1)}, u32[]{:S(2)}, u32[]{:S(2)}) collective-permute-start(bf16[256,2048]{1,0:T(8,128)(2,1)S(1)} %multiply_convert_fusion.2), channel_id=1, source_target_pairs={{0,1},{1,0},{2,3},{3,2},{4,5},{5,4},{6,7},{7,6},{8,9},{9,8},{10,11... | collective-permute-start | bytes 3145736 | tf_op jit(solution)/shard_map/ppermute | solution.py:35
  43.6 22.8 %collective-permute-start.2 = (bf16[256,2048]{1,0:T(8,128)(2,1)}, bf16[256,2048]{1,0:T(8,128)(2,1)}, u32[]{:S(2)}, u32[]{:S(2)}) collective-permute-start(bf16[256,2048]{1,0:T(8,128)(2,1)} %collective-permute-done), channel_id=1, source_target_pairs={{0,1},{1,0},{2,3},{3,2},{4,5},{5,4},{6,7},{7,6},{8,9},{9,8},{10,11... | collective-permute-start | bytes 3145736 | tf_op jit(solution)/shard_map/ppermute | solution.py:35
  44.8 255.5 %all-gather.23.cloned.1.call-start = ((), (), s32[]{:S(2)}) async-start(), calls=%async_computation.5 | async-start | bytes 2621440 | tf_op jit(solution)/shard_map/all_gather | solution.py:94
  64.9 105.2 %collective-permute-start.3 = (bf16[3,256,1152]{2,1,0:T(8,128)(2,1)}, bf16[3,256,1152]{2,1,0:T(8,128)(2,1)}, u32[]{:S(2)}, u32[]{:S(2)}) collective-permute-start(bf16[3,256,1152]{2,1,0:T(8,128)(2,1)} %pad_maximum_fusion.8), channel_id=1, source_target_pairs={{0,16},{16,0},{1,17},{17,1},{2,18},{18,2},{3,19},{19,3},{4,20},{20... | collective-permute-start | bytes 5308424 | tf_op jit(solution)/shard_map/ppermute | solution.py:108
  117.8 57.1 %collective-permute-start.4 = (bf16[768,1152]{1,0:T(8,128)(2,1)}, bf16[768,1152]{1,0:T(8,128)(2,1)}, u32[]{:S(2)}, u32[]{:S(2)}) collective-permute-start(bf16[768,1152]{1,0:T(8,128)(2,1)} %fusion.20), channel_id=1, source_target_pairs={{0,16},{16,0},{1,17},{17,1},{2,18},{18,2},{3,19},{19,3},{4,20},{20... | collective-permute-start | bytes 5308424 | tf_op jit(solution)/shard_map/ppermute | solution.py:108
  162.6 4.7 %copy-start.20 = (bf16[1024,2048]{1,0:T(8,128)(2,1)S(1)}, bf16[1024,2048]{1,0:T(8,128)(2,1)}, u32[]{:S(2)}) copy-start(bf16[1024,2048]{1,0:T(8,128)(2,1)} %pad_maximum_fusion) | copy-start | bytes 12582916
  164.3 3.0 copy-start.31
  165.8 4.4 %copy-start.26 = (bf16[1,256,1152]{2,1,0:T(8,128)(2,1)S(1)}, bf16[1,256,1152]{2,1,0:T(8,128)(2,1)}, u32[]{:S(2)}) copy-start(bf16[1,256,1152]{2,1,0:T(8,128)(2,1)} %get-tuple-element.18) | copy-start | bytes 1769476
  165.8 40.5 %collective-permute-start.7 = (bf16[3,1152,256]{2,1,0:T(8,128)(2,1)}, bf16[3,1152,256]{2,1,0:T(8,128)(2,1)}, u32[]{:S(2)}, u32[]{:S(2)}) collective-permute-start(bf16[3,1152,256]{2,1,0:T(8,128)(2,1)} %pad_maximum_fusion.9), channel_id=1, source_target_pairs={{0,16},{16,0},{1,17},{17,1},{2,18},{18,2},{3,19},{19,3},{4,20},{20... | collective-permute-start | bytes 5308424 | tf_op jit(solution)/shard_map/ppermute | solution.py:108
  171.9 2.9 copy-start.27
  176.6 2.9 copy-start.15
  184.2 22.1 %copy-start.25 = (bf16[1,1152,256]{2,1,0:T(8,128)(2,1)S(1)}, bf16[1,1152,256]{2,1,0:T(8,128)(2,1)}, u32[]{:S(2)}) copy-start(bf16[1,1152,256]{2,1,0:T(8,128)(2,1)} %get-tuple-element.16) | copy-start | bytes 1769476
  189.3 36.1 %collective-permute-start.5 = (bf16[512,1024]{1,0:T(8,128)(2,1)}, bf16[512,1024]{1,0:T(8,128)(2,1)}, u32[]{:S(2)}, u32[]{:S(2)}) collective-permute-start(bf16[512,1024]{1,0:T(8,128)(2,1)} %shard_map.119), channel_id=1, source_target_pairs={{0,1},{1,0},{2,3},{3,2},{4,5},{5,4},{6,7},{7,6},{8,9},{9,8},{10,11... | collective-permute-start | bytes 3145736 | tf_op jit(solution)/shard_map/ppermute | solution.py:35
  214.4 14.2 %collective-permute-start.8 = (bf16[512,1024]{1,0:T(8,128)(2,1)}, bf16[512,1024]{1,0:T(8,128)(2,1)}, u32[]{:S(2)}, u32[]{:S(2)}) collective-permute-start(bf16[512,1024]{1,0:T(8,128)(2,1)} %shard_map.121), channel_id=1, source_target_pairs={{0,1},{1,0},{2,3},{3,2},{4,5},{5,4},{6,7},{7,6},{8,9},{9,8},{10,11... | collective-permute-start | bytes 3145736 | tf_op jit(solution)/shard_map/ppermute | solution.py:35
  220.1 5.2 %copy-start.24 = (bf16[512,1024]{1,0:T(8,128)(2,1)S(1)}, bf16[512,1024]{1,0:T(8,128)(2,1)}, u32[]{:S(2)}) copy-start(bf16[512,1024]{1,0:T(8,128)(2,1)} %shard_map.118) | copy-start | bytes 3145732
  225.3 3.3 copy-start.23
  227.0 3.2 copy-start.11
  227.1 5.6 %copy-start.37 = (bf16[1024,512]{1,0:T(8,128)(2,1)S(1)}, bf16[1024,512]{1,0:T(8,128)(2,1)}, u32[]{:S(2)}) copy-start(bf16[1024,512]{1,0:T(8,128)(2,1)} %param.22) | copy-start | bytes 3145732
  227.1 15.0 %collective-permute-start.6 = (bf16[256,1024]{1,0:T(8,128)(2,1)S(1)}, bf16[256,1024]{1,0:T(8,128)(2,1)}, u32[]{:S(2)}, u32[]{:S(2)}) collective-permute-start(bf16[256,1024]{1,0:T(8,128)(2,1)S(1)} %slice.161), channel_id=1, source_target_pairs={{2,0},{3,1},{0,2},{1,3},{6,4},{7,5},{4,6},{5,7},{10,8},{11,9},{8,1... | collective-permute-start | bytes 1572872 | tf_op jit(solution)/shard_map/ppermute | solution.py:31
  231.8 21.1 %collective-permute-start.9 = (bf16[256,1024]{1,0:T(8,128)(2,1)}, bf16[256,1024]{1,0:T(8,128)(2,1)}, u32[]{:S(2)}, u32[]{:S(2)}) collective-permute-start(bf16[256,1024]{1,0:T(8,128)(2,1)} %slice.160), channel_id=1, source_target_pairs={{2,0},{3,1},{0,2},{1,3},{6,4},{7,5},{4,6},{5,7},{10,8},{11,9},{8,1... | collective-permute-start | bytes 1572872 | tf_op jit(solution)/shard_map/ppermute | solution.py:31
  233.8 8.3 %copy-start.12 = (f32[512,1024]{1,0:T(8,128)S(1)}, f32[512,1024]{1,0:T(8,128)}, u32[]{:S(2)}) copy-start(f32[512,1024]{1,0:T(8,128)} %copy-done.11) | copy-start | bytes 6291460
  233.9 19.0 %copy-start.14 = (f32[512,1024]{1,0:T(8,128)S(1)}, f32[512,1024]{1,0:T(8,128)}, u32[]{:S(2)}) copy-start(f32[512,1024]{1,0:T(8,128)} %copy-done.13) | copy-start | bytes 6291460
  243.4 10.8 %copy-start.4 = (bf16[256,4,1,256]{3,0,2,1:T(8,128)(2,1)S(1)}, bf16[256,4,1,256]{3,0,2,1:T(8,128)(2,1)}, u32[]{:S(2)}) copy-start(bf16[256,4,1,256]{3,0,2,1:T(8,128)(2,1)} %copy-done.3) | copy-start | bytes 1572868
  243.4 10.8 %copy-start.6 = (bf16[256,4,256]{2,0,1:T(8,128)(2,1)S(1)}, bf16[256,4,256]{2,0,1:T(8,128)(2,1)}, u32[]{:S(2)}) copy-start(bf16[256,4,256]{2,0,1:T(8,128)(2,1)} %copy-done.5) | copy-start | bytes 1572868
  255.1 2.8 copy-start.16
  255.1 2.8 slice-start.2
  256.4 25.1 %collective-permute-start.10 = (bf16[256,2048]{1,0:T(8,128)(2,1)}, bf16[256,2048]{1,0:T(8,128)(2,1)}, u32[]{:S(2)}, u32[]{:S(2)}) collective-permute-start(bf16[256,2048]{1,0:T(8,128)(2,1)} %multiply_convert_fusion.1), channel_id=1, source_target_pairs={{2,0},{3,1},{0,2},{1,3},{6,4},{7,5},{4,6},{5,7},{10,8},{11,9},{8,1... | collective-permute-start | bytes 3145736 | tf_op jit(solution)/shard_map/ppermute | solution.py:31
  260.8 47.5 %collective-permute-start.13 = (bf16[768,1024]{1,0:T(8,128)(2,1)}, bf16[768,1024]{1,0:T(8,128)(2,1)}, u32[]{:S(2)}, u32[]{:S(2)}) collective-permute-start(bf16[768,1024]{1,0:T(8,128)(2,1)} %fusion.22), channel_id=1, source_target_pairs={{0,16},{16,0},{1,17},{17,1},{2,18},{18,2},{3,19},{19,3},{4,20},{20... | collective-permute-start | bytes 4718600 | tf_op jit(solution)/shard_map/ppermute | solution.py:108
  265.2 66.8 %collective-permute-start.14 = (bf16[3,256,1024]{2,1,0:T(8,128)(2,1)}, bf16[3,256,1024]{2,1,0:T(8,128)(2,1)}, u32[]{:S(2)}, u32[]{:S(2)}) collective-permute-start(bf16[3,256,1024]{2,1,0:T(8,128)(2,1)} %pad_maximum_fusion.10), channel_id=1, source_target_pairs={{0,16},{16,0},{1,17},{17,1},{2,18},{18,2},{3,19},{19,3},{4,20},{20... | collective-permute-start | bytes 4718600 | tf_op jit(solution)/shard_map/ppermute | solution.py:108
  265.8 67.9 %collective-permute-start.11 = (bf16[256,2048]{1,0:T(8,128)(2,1)}, bf16[256,2048]{1,0:T(8,128)(2,1)}, u32[]{:S(2)}, u32[]{:S(2)}) collective-permute-start(bf16[256,2048]{1,0:T(8,128)(2,1)} %multiply_convert_fusion.1), channel_id=1, source_target_pairs={{0,1},{1,0},{2,3},{3,2},{4,5},{5,4},{6,7},{7,6},{8,9},{9,8},{10,11... | collective-permute-start | bytes 3145736 | tf_op jit(solution)/shard_map/ppermute | solution.py:35
  281.5 52.2 %collective-permute-start.12 = (bf16[256,2048]{1,0:T(8,128)(2,1)}, bf16[256,2048]{1,0:T(8,128)(2,1)}, u32[]{:S(2)}, u32[]{:S(2)}) collective-permute-start(bf16[256,2048]{1,0:T(8,128)(2,1)} %collective-permute-done.10), channel_id=1, source_target_pairs={{0,1},{1,0},{2,3},{3,2},{4,5},{5,4},{6,7},{7,6},{8,9},{9,8},{10,11... | collective-permute-start | bytes 3145736 | tf_op jit(solution)/shard_map/ppermute | solution.py:35
  301.5 6.7 %copy-start.28 = (bf16[1,256,1024]{2,1,0:T(8,128)(2,1)S(1)}, bf16[1,256,1024]{2,1,0:T(8,128)(2,1)}, u32[]{:S(2)}) copy-start(bf16[1,256,1024]{2,1,0:T(8,128)(2,1)} %get-tuple-element.30) | copy-start | bytes 1572868
  306.8 58.4 %collective-permute-start.17 = (bf16[3072,256]{1,0:T(8,128)(2,1)}, bf16[3072,256]{1,0:T(8,128)(2,1)}, u32[]{:S(2)}, u32[]{:S(2)}) collective-permute-start(bf16[3072,256]{1,0:T(8,128)(2,1)} %fusion.21), channel_id=1, source_target_pairs={{0,16},{16,0},{1,17},{17,1},{2,18},{18,2},{3,19},{19,3},{4,20},{20... | collective-permute-start | bytes 4718600 | tf_op jit(solution)/shard_map/ppermute | solution.py:108
  308.2 23.8 %copy-start.29 = (bf16[1,256,1024]{2,1,0:T(8,128)(2,1)S(1)}, bf16[1,256,1024]{2,1,0:T(8,128)(2,1)}, u32[]{:S(2)}) copy-start(bf16[1,256,1024]{2,1,0:T(8,128)(2,1)} %get-tuple-element.26) | copy-start | bytes 1572868
  336.3 2.3 copy-start.32
  342.3 2.3 copy-start.17
  360.3 4.9 %copy-start.30 = (bf16[1,1024,256]{2,1,0:T(8,128)(2,1)S(1)}, bf16[1,1024,256]{2,1,0:T(8,128)(2,1)}, u32[]{:S(2)}) copy-start(bf16[1,1024,256]{2,1,0:T(8,128)(2,1)} %get-tuple-element.24) | copy-start | bytes 1572868
  365.1 18.1 %collective-permute-start.15 = (bf16[512,1024]{1,0:T(8,128)(2,1)}, bf16[512,1024]{1,0:T(8,128)(2,1)S(1)}, u32[]{:S(2)}, u32[]{:S(2)}) collective-permute-start(bf16[512,1024]{1,0:T(8,128)(2,1)} %shard_map.123), channel_id=1, source_target_pairs={{0,1},{1,0},{2,3},{3,2},{4,5},{5,4},{6,7},{7,6},{8,9},{9,8},{10,11... | collective-permute-start | bytes 3145736 | tf_op jit(solution)/shard_map/ppermute | solution.py:35
  372.8 12.8 %collective-permute-start.18 = (bf16[512,1024]{1,0:T(8,128)(2,1)}, bf16[512,1024]{1,0:T(8,128)(2,1)}, u32[]{:S(2)}, u32[]{:S(2)}) collective-permute-start(bf16[512,1024]{1,0:T(8,128)(2,1)} %shard_map.125), channel_id=1, source_target_pairs={{0,1},{1,0},{2,3},{3,2},{4,5},{5,4},{6,7},{7,6},{8,9},{9,8},{10,11... | collective-permute-start | bytes 3145736 | tf_op jit(solution)/shard_map/ppermute | solution.py:35
  378.1 5.1 %copy-start.22 = (bf16[512,1024]{1,0:T(8,128)(2,1)S(1)}, bf16[512,1024]{1,0:T(8,128)(2,1)}, u32[]{:S(2)}) copy-start(bf16[512,1024]{1,0:T(8,128)(2,1)} %shard_map.122) | copy-start | bytes 3145732
  383.3 2.4 copy-start.21
  383.7 3.5 copy-start.7
  384.7 15.1 %collective-permute-start.16 = (bf16[256,1024]{1,0:T(8,128)(2,1)}, bf16[256,1024]{1,0:T(8,128)(2,1)}, u32[]{:S(2)}, u32[]{:S(2)}) collective-permute-start(bf16[256,1024]{1,0:T(8,128)(2,1)} %slice.159), channel_id=1, source_target_pairs={{2,0},{3,1},{0,2},{1,3},{6,4},{7,5},{4,6},{5,7},{10,8},{11,9},{8,1... | collective-permute-start | bytes 1572872 | tf_op jit(solution)/shard_map/ppermute | solution.py:31
  387.2 3.1 copy-start.1
  388.7 21.4 %collective-permute-start.19 = (bf16[256,1024]{1,0:T(8,128)(2,1)}, bf16[256,1024]{1,0:T(8,128)(2,1)}, u32[]{:S(2)}, u32[]{:S(2)}) collective-permute-start(bf16[256,1024]{1,0:T(8,128)(2,1)} %slice.158), channel_id=1, source_target_pairs={{2,0},{3,1},{0,2},{1,3},{6,4},{7,5},{4,6},{5,7},{10,8},{11,9},{8,1... | collective-permute-start | bytes 1572872 | tf_op jit(solution)/shard_map/ppermute | solution.py:31
  391.8 8.0 %copy-start.8 = (f32[512,1024]{1,0:T(8,128)S(1)}, f32[512,1024]{1,0:T(8,128)}, u32[]{:S(2)}) copy-start(f32[512,1024]{1,0:T(8,128)} %copy-done.7) | copy-start | bytes 6291460
  402.0 8.1 %copy-start.10 = (f32[512,1024]{1,0:T(8,128)S(1)}, f32[512,1024]{1,0:T(8,128)}, u32[]{:S(2)}) copy-start(f32[512,1024]{1,0:T(8,128)} %copy-done.9) | copy-start | bytes 6291460
  412.3 4.4 %copy-start.2 = (f32[256,8,256]{2,0,1:T(8,128)S(1)}, f32[256,8,256]{2,0,1:T(8,128)}, u32[]{:S(2)}) copy-start(f32[256,8,256]{2,0,1:T(8,128)} %get-tuple-element.22) | copy-start | bytes 6291460
  415.1 1.6 copy-start.18
  415.1 1.9 copy-start.19
  (7 other events, 9.0 us)
Sparse Core Ops, SparseCore 0:
  9.2 52.6 all-gather.12
  63.5 48.7 all-gather.14
  113.8 48.7 all-gather.16
  164.0 44.4 all-gather.18
  209.9 44.4 all-gather.20
  255.8 44.4 all-gather.22
